TPU v7x, 32 devices: a whole 2x2x4 slice. The times are simulated.
32 devices in a mesh: grp: 2 (over y), ep: 4 (over z), tp: 4 (over x, core).
Axes of the slice: x: 2, y: 2, z: 4, core: 2. Of those that a mesh axis runs over, the one named last changes fastest.
Arguments:
- mix_input: bfloat16 [2048, 2048], P(('grp', 'ep'), 'tp'), parts along dimension 0, may hold values from -6 to 6
- group_weight: bfloat16 [16, 128, 128], replicated, may hold values from -0.5 to 0.5
- pool_gain: float32 [2048], replicated, may hold values from 0.1 to 1.9
- branch_weight: bfloat16 [2048, 2048], P('tp'), may hold values from -0.125 to 0.125
- exp_input: bfloat16 [1024, 2048], P(('grp', 'ep')), parts along dimension 0, may hold values from -6 to 6
- norm_gain: float32 [2048], replicated, may hold values from 0.1 to 1.9
- routes: int32 [1024, 2], P(('grp', 'ep')), parts along dimension 0, may hold values from 0 to 3, all different within a row; in each aligned block of 128 rows (0 to 127, 128 to 255, ...) at most 96 rows name the same one
- route_weights: float32 [1024, 2], P(('grp', 'ep')), parts along dimension 0, may hold values from 0.25 to 1
- gate_weight: bfloat16 [4, 2048, 3584], P('ep', None, 'tp'), may hold values from -0.125 to 0.125
- up_weight: bfloat16 [4, 2048, 3584], P('ep', None, 'tp'), may hold values from -0.125 to 0.125
- down_weight: bfloat16 [4, 3584, 2048], P('ep', 'tp'), may hold values from -0.09375 to 0.09375
Outputs:
- mix_out: bfloat16 [2048, 2048], P(('grp', 'ep'), 'tp'), parts along dimension 0
- exp_out: bfloat16 [1024, 2048], P(('grp', 'ep'), 'tp'), parts along dimension 0
There are 2 independent parts, one for each index of `grp`. A program takes and returns all parts, laid end to end along the dimension named above; an argument that names none is the same for every part. Nothing has to cross between parts.
Inputs may be any that keep to these rules, and one draw needn't show every extreme that they name: `routes`: the 2 experts of a token differ. Among the 128 tokens of one index of ep no expert is named by more than 96 of them, a bound that some block reaches.
All inputs are finite; a program needn't handle non-finite values.
Results may differ from a plain program's by a relative error of at most 0.018.
Values may be sent and summed in bfloat16 or wider, within the bound.
A program may use at most 64 MiB of HBM per device.

v0:
```python
import jax
import jax.numpy as jnp
from jax import lax
from jax.sharding import PartitionSpec as P

windows = (2, 4, 8, 16)
epsilon = 1e-06


def shifted(block, axis, distance):
    devices = range(lax.axis_size(axis))
    route = [(i - distance, i) for i in devices if i - distance in devices]
    return lax.ppermute(block, axis, route)


def trailing_sums(extended, rows):
    span_two = extended[1:] + extended[:-1]
    span_four = span_two[2:] + span_two[:-2]
    span_eight = span_four[4:] + span_four[:-4]
    span_sixteen = span_eight[8:] + span_eight[:-8]
    return [span_two[-rows:], span_four[-rows:], span_eight[-rows:], span_sixteen]


def pooled_deviation(extended, positions, group_ids, group_width, rows):
    sums = trailing_sums(extended, rows)
    current = extended[-rows:]
    window_id = jnp.repeat(group_ids % 4, group_width)
    result = jnp.zeros_like(current)
    for window_level, window_len in enumerate(windows):
        counted = jnp.minimum(positions + 1, window_len).astype(jnp.float32)[:, None]
        result = jnp.where(
            window_id[None, :] == window_level, sums[window_level] / counted - current, result
        )
    return result


def on_device(
    mix_input,
    group_weight,
    pool_gain,
    branch_weight,
    exp_input,
    norm_gain,
    routes,
    route_weights,
    gate_weight,
    up_weight,
    down_weight,
):
    tp_rank = lax.axis_index("tp")
    ep_rank = lax.axis_index("ep")
    rows_mix, channels = mix_input.shape
    group_width = group_weight.shape[1]
    group_count = channels // group_width
    first_group = tp_rank * group_count
    last_rows = mix_input[rows_mix - 15 :]
    before = shifted(last_rows, "ep", 1)
    extended = jnp.concatenate([before, mix_input], axis=0).astype(jnp.float32)
    positions = ep_rank * rows_mix + jnp.arange(rows_mix, dtype=jnp.int32)
    group_ids = first_group + jnp.arange(group_count, dtype=jnp.int32)
    deviation = pooled_deviation(extended, positions, group_ids, group_width, rows_mix).astype(
        jnp.bfloat16
    )
    own_groups = lax.dynamic_slice_in_dim(group_weight, first_group, group_count, 0)
    grouped = jnp.einsum(
        "rgc,gcd->rgd",
        deviation.reshape(rows_mix, group_count, group_width),
        own_groups,
        preferred_element_type=jnp.float32,
    ).reshape(rows_mix, channels)
    own_gain = lax.dynamic_slice_in_dim(pool_gain, first_group * group_width, channels, 0)
    pooled = (grouped * own_gain).astype(jnp.bfloat16)
    tok_rows, width = exp_input.shape
    columns = width // lax.axis_size("tp")
    experts_all = lax.axis_size("ep")
    capacity = 3 * tok_rows // experts_all
    floated = exp_input.astype(jnp.float32)
    normed = (
        floated
        * lax.rsqrt(jnp.mean(floated * floated, axis=1, keepdims=True) + epsilon)
        * norm_gain
    ).astype(jnp.bfloat16)
    flat_expert = routes.reshape(-1)
    assignments = flat_expert.shape[0]
    onehot = (flat_expert[:, None] == jnp.arange(experts_all, dtype=jnp.int32)[None, :]).astype(
        jnp.int32
    )
    slot_rank = jnp.sum((jnp.cumsum(onehot, axis=0) - onehot) * onehot, axis=1)
    slot_index = flat_expert * capacity + slot_rank
    token_of = jnp.arange(assignments, dtype=jnp.int32) // routes.shape[1]
    slot_token = (
        jnp.full((experts_all * capacity,), tok_rows, jnp.int32).at[slot_index].set(token_of)
    )
    padded = jnp.concatenate([normed, jnp.zeros((1, width), jnp.bfloat16)], axis=0)
    w_gate = gate_weight[0]
    w_up = up_weight[0]
    w_down = down_weight[0]
    arrived_rows = experts_all * capacity
    own_columns = lax.dynamic_slice_in_dim(padded, tp_rank * columns, columns, 1)
    outgoing = own_columns[slot_token].reshape(experts_all, capacity, columns)
    arrived = lax.all_to_all(outgoing, "ep", split_axis=0, concat_axis=0, tiled=True).reshape(
        arrived_rows, columns
    )
    section = lax.all_gather(arrived, "tp", axis=1, tiled=True)
    gate_pre = jnp.dot(section, w_gate, preferred_element_type=jnp.float32)
    up_pre = jnp.dot(section, w_up, preferred_element_type=jnp.float32)
    hidden = (jax.nn.silu(gate_pre) * up_pre).astype(jnp.bfloat16)
    weight_cols = branch_weight
    mix_sum = lax.psum_scatter(
        lax.dot_general(
            weight_cols, pooled, (((0,), (1,)), ((), ())), preferred_element_type=jnp.float32
        ).astype(jnp.bfloat16),
        "tp",
        scatter_dimension=0,
        tiled=True,
    )
    weight_cols = w_down
    exp_sum = lax.psum_scatter(
        lax.dot_general(
            weight_cols, hidden, (((0,), (1,)), ((), ())), preferred_element_type=jnp.float32
        ).astype(jnp.bfloat16),
        "tp",
        scatter_dimension=0,
        tiled=True,
    )
    mix_out = mix_sum.T
    results = exp_sum.reshape(columns, experts_all, capacity)
    returned = lax.all_to_all(results, "ep", split_axis=1, concat_axis=1, tiled=True).reshape(
        columns, experts_all * capacity
    )
    picked = returned[:, slot_index].astype(jnp.float32)
    weighted = picked * route_weights.reshape(-1)[None, :]
    combined = jnp.sum(weighted.reshape(columns, tok_rows, routes.shape[1]), axis=2)
    exp_out = combined.T.astype(jnp.bfloat16)
    return (mix_out, exp_out)


def solution(mesh):
    return jax.shard_map(
        on_device,
        mesh=mesh,
        in_specs=(
            P(("grp", "ep"), "tp"),
            P(),
            P(),
            P("tp", None),
            P(("grp", "ep"), None),
            P(),
            P(("grp", "ep"), None),
            P(("grp", "ep"), None),
            P("ep", None, "tp"),
            P("ep", None, "tp"),
            P("ep", "tp", None),
        ),
        out_specs=(P(("grp", "ep"), "tp"), P(("grp", "ep"), "tp")),
        check_vma=False,
    )
```

profile of v0, /device:TPU:0, one launch (start us, length us, event | category | flops | bytes accessed | tf_op | source)
XLA Modules:
  0.0 130.7 jit_solution(4550041975561271826)
XLA Ops:
  7.2 0.9 copy.21
  8.3 0.1 eq.93
  8.4 0.7 broadcast_multiply_fusion
  9.1 1.2 fusion.19
  10.4 1.2 reduce-window.6
  12.1 0.1 mul.84
  12.3 1.4 %scatter_custom_fusion = s32[384]{0:T(512)S(1)} fusion(s32[256]{0:T(256)S(1)} %bitcast.86, s32[256]{0:T(256)S(1)} %and_select_fusion, s32[]{:T(128)} %constant.80.clone.1), kind=kCustom, calls=%fused_computation.66 | custom fusion | bytes 1540 | tf_op jit(solution)/shard_map/scatter | solution.py:92
  13.7 1.2 fusion.21
  15.0 2.1 %gather_fusion = bf16[384,512]{1,0:T(8,128)(2,1)S(1)} fusion(bf16[129,512]{1,0:T(8,128)(2,1)S(1)} %pad_dynamic-slice_fusion, s32[1024]{0:T(1024)S(1)} %pad_clamp_fusion.1), kind=kCustom, calls=%fused_computation | custom fusion | bytes 787968 | tf_op jit(solution)/shard_map/gather | solution.py:100
  17.1 17.9 %all_to_all.10 = bf16[4,96,512]{2,1,0:T(8,128)(2,1)} all-to-all(bf16[4,96,512]{2,1,0:T(8,128)(2,1)S(1)} %bitcast.83), channel_id=1, replica_groups=mesh['grp'=2,'ep'=4,'tp'=4] {'ep'}, dimensions={0} | all-to-all | bytes 786432 | tf_op jit(solution)/shard_map/all_to_all | solution.py:101
  35.1 2.1 %collective-permute-start = (bf16[15,512]{1,0:T(8,128)(2,1)S(1)}, bf16[15,512]{1,0:T(8,128)(2,1)S(1)}, u32[]{:S(2)}, u32[]{:S(2)}) collective-permute-start(bf16[15,512]{1,0:T(8,128)(2,1)S(1)} %slice.43), channel_id=1, source_target_pairs={{0,4},{4,8},{8,12},{1,5},{5,9},{9,13},{2,6},{6,10},{10,14},{3,7},{... | collective-permute-start | bytes 46088 | tf_op jit(solution)/shard_map/ppermute | solution.py:13
  37.2 16.7 %all-gather.2.cloned.1.call-done = bf16[384,2048]{1,0:T(8,128)(2,1)} async-done(((bf16[384,512]{1,0:T(8,128)(2,1)}), bf16[384,2048]{1,0:T(8,128)(2,1)}) %all-gather.2.cloned.1.call-update) | async-done | bytes 1572880 | tf_op jit(solution)/shard_map/all_gather | solution.py:104
  53.9 5.4 %fusion.4 = f32[384,896]{1,0:T(8,128)} fusion(bf16[384,2048]{1,0:T(8,128)(2,1)} %all-gather.2.cloned.1.call-done, bf16[1,2048,896]{2,1,0:T(8,128)(2,1)} %param.19), kind=kOutput, calls=%fused_computation.7 | convolution fusion | flops 1409286144 | bytes 6619136 | tf_op jit(solution)/shard_map/dot_general | solution.py:105
  59.3 8.6 %fusion.9 = bf16[2048,384]{0,1:T(8,128)(2,1)} fusion(bf16[1,896,2048]{2,1,0:T(8,128)(2,1)} %param.21, bf16[384,2048]{1,0:T(8,128)(2,1)} %all-gather.2.cloned.1.call-done, bf16[1,2048,896]{2,1,0:T(8,128)(2,1)} %param.20, f32[384,896]{1,0:T(8,128)} %fusion.4), kind=kOutput, calls=%fused_computation.10 | convolution fusion | flops 2821423104 | bytes 11862016 | tf_op jit(solution)/shard_map/dot_general | solution.py:119
  68.4 0.8 dynamic_slice.10
  69.4 1.5 %fusion.35 = f32[4,128,256]{2,1,0:T(8,128)S(1)} fusion(bf16[16,128,128]{2,1,0:T(8,128)(2,1)} %param.12, s32[]{:T(128)S(6)} %select_n.46, f32[256]{0:T(256)S(1)} %get-tuple-element.2, f32[270,512]{1,0:T(8,128)S(1)} %slice_add_fusion.1, pred[512]{0:T(512)(128)(4,1)S(1)} %broadcast_bitcast_fusion, f32[256]{0:T(256)S(1)} %get-tuple-element.3, ...), kind=kOutput, calls=%fused_computation.42 | convolution fusion | flops 35389440 | bytes 3282948 | tf_op jit(solution)/shard_map/rgc,gcd->rgd/dot_general | solution.py:65
  71.1 1.7 %fusion.12 = bf16[2048,256]{0,1:T(8,128)(2,1)} fusion(bf16[256,512]{0,1:T(8,128)(2,1)S(1)} %fusion.33, bf16[512,2048]{1,0:T(8,128)(2,1)S(1)} %copy-done), kind=kOutput, calls=%fused_computation.12 | convolution fusion | flops 537395200 | bytes 3407872 | tf_op jit(solution)/shard_map/dot_general | solution.py:110
  72.8 23.4 %reduce-scatter.5.cloned.1.call-done = bf16[512,384]{0,1:T(8,128)(2,1)} async-done(((bf16[2048,384]{0,1:T(8,128)(2,1)}), bf16[512,384]{0,1:T(8,128)(2,1)}) %reduce-scatter.5.cloned.1.call-update) | async-done | bytes 393232 | tf_op jit(solution)/shard_map/reduce_scatter | solution.py:118
  96.2 4.6 %all-to-all-start.1 = ((bf16[512,4,96]{0,2,1:T(8,128)(2,1)}), bf16[512,4,96]{0,2,1:T(8,128)(2,1)S(1)}, u32[]{:S(2)}, u32[]{:S(2)}) async-start(bf16[512,4,96]{0,2,1:T(8,128)(2,1)} %bitcast.84), calls=%async_computation.3 | async-start | bytes 786432 | tf_op jit(solution)/shard_map/all_to_all | solution.py:128
  100.9 11.4 %all-to-all-done.1 = bf16[512,4,96]{0,2,1:T(8,128)(2,1)S(1)} async-done(((bf16[512,4,96]{0,2,1:T(8,128)(2,1)}), bf16[512,4,96]{0,2,1:T(8,128)(2,1)S(1)}, u32[]{:S(2)}, u32[]{:S(2)}) %all-to-all-start.1) | async-done | bytes 393248 | tf_op jit(solution)/shard_map/all_to_all | solution.py:128
  112.3 1.2 gather_fusion.1
  113.5 0.3 reshape.150
  113.8 1.4 %multiply_reduce_fusion = bf16[512,128]{0,1:T(8,128)(2,1)} fusion(f32[512,128,2]{0,2,1:T(2,128)S(1)} %reshape.150, f32[128,2]{1,0:T(8,128)S(1)} %copy.25), kind=kLoop, calls=%fused_computation.39 | loop fusion | flops 196608 | bytes 656384 | tf_op jit(solution)/shard_map/reduce_sum | solution.py:133
  115.2 8.9 %reduce-scatter.3.cloned.1.call-done = bf16[512,256]{0,1:T(8,128)(2,1)} async-done(((bf16[2048,256]{0,1:T(8,128)(2,1)}), bf16[512,256]{0,1:T(8,128)(2,1)}) %reduce-scatter.3.cloned.1.call-update) | async-done | bytes 262160 | tf_op jit(solution)/shard_map/reduce_scatter | solution.py:109
  (46 shorter events, 1.8 us)
Async XLA Ops:
  7.2 63.9 %copy-start = (bf16[512,2048]{1,0:T(8,128)(2,1)S(1)}, bf16[512,2048]{1,0:T(8,128)(2,1)}, u32[]{:S(2)}) copy-start(bf16[512,2048]{1,0:T(8,128)(2,1)} %param.14) | copy-start | bytes 6291460
  7.2 46.7 %all-gather.2.cloned.1.call-start = ((), (), s32[]{:S(2)}) async-start(), calls=%async_computation.5 | async-start | bytes 1966080 | tf_op jit(solution)/shard_map/all_gather | solution.py:104
  15.0 20.1 %copy-start.1 = (bf16[256,512]{1,0:T(8,128)(2,1)S(1)}, bf16[256,512]{1,0:T(8,128)(2,1)}, u32[]{:S(2)}) copy-start(bf16[256,512]{1,0:T(8,128)(2,1)} %param.11) | copy-start | bytes 786436
  35.0 61.2 %reduce-scatter.5.cloned.1.call-start = ((), (), s32[]{:S(2)}) async-start(), calls=%async_computation.6 | async-start | bytes 1966080 | tf_op jit(solution)/shard_map/reduce_scatter | solution.py:118
  35.1 34.0 %collective-permute-start = (bf16[15,512]{1,0:T(8,128)(2,1)S(1)}, bf16[15,512]{1,0:T(8,128)(2,1)S(1)}, u32[]{:S(2)}, u32[]{:S(2)}) collective-permute-start(bf16[15,512]{1,0:T(8,128)(2,1)S(1)} %slice.43), channel_id=1, source_target_pairs={{0,4},{4,8},{8,12},{1,5},{5,9},{9,13},{2,6},{6,10},{10,14},{3,7},{... | collective-permute-start | bytes 46088 | tf_op jit(solution)/shard_map/ppermute | solution.py:13
  67.9 56.2 %reduce-scatter.3.cloned.1.call-start = ((), (), s32[]{:S(2)}) async-start(), calls=%async_computation.4 | async-start | bytes 1310720 | tf_op jit(solution)/shard_map/reduce_scatter | solution.py:109
  72.8 28.0 %copy-start.2 = (f32[128,2]{0,1:T(2,128)S(1)}, f32[128,2]{0,1:T(2,128)}, u32[]{:S(2)}) copy-start(f32[128,2]{0,1:T(2,128)} %param.18) | copy-start | bytes 3076
  96.2 16.1 %all-to-all-start.1 = ((bf16[512,4,96]{0,2,1:T(8,128)(2,1)}), bf16[512,4,96]{0,2,1:T(8,128)(2,1)S(1)}, u32[]{:S(2)}, u32[]{:S(2)}) async-start(bf16[512,4,96]{0,2,1:T(8,128)(2,1)} %bitcast.84), calls=%async_computation.3 | async-start | bytes 786432 | tf_op jit(solution)/shard_map/all_to_all | solution.py:128
Sparse Core Ops, SparseCore 0:
  35.1 18.7 all-gather.1
  68.1 28.0 reduce-scatter.4
  99.3 24.7 reduce-scatter.2
where the time goes:
time: 131 us
  waiting for transfers between devices  60.4 us (46%)
  blocking collectives  17.9 us (14%)
  matrix products  17.2 us (13%)
  between operations  14 us (11%)
  local copies, waits for them, and re-layouts  7.86 us (6%)
  starting transfers between devices  6.83 us (5%)
  other arithmetic  6.43 us (5%)
    reduce_scatter x1, waiting for transfers between devices, on_device(): lax.psum_scatter(lax.dot_general(weight_cols, hidden, (((0,), (1,)), ((),...  23.4 us
    all_to_all x1, blocking collectives, on_device(): lax.all_to_all(outgoing, 'ep', split_axis=0, concat_axis=0, tiled=True)  17.9 us
    all_gather x1, waiting for transfers between devices, on_device(): section = lax.all_gather(arrived, 'tp', axis=1, tiled=True)  16.7 us
    all_to_all x1, waiting for transfers between devices, on_device(): lax.all_to_all(results, 'ep', split_axis=1, concat_axis=1, tiled=True)  11.4 us
    reduce_scatter x1, waiting for transfers between devices, on_device(): lax.psum_scatter(lax.dot_general(weight_cols, pooled, (((0,), (1,)), ((),...  8.93 us
    dot_general x1, matrix products, on_device(): lax.dot_general(weight_cols, hidden, (((0,), (1,)), ((), ())), preferred_...  8.61 us
    dot_general x1, matrix products, on_device(): gate_pre = jnp.dot(section, w_gate, preferred_element_type=jnp.float32)  5.4 us
    all_to_all x1, starting transfers between devices, on_device(): lax.all_to_all(results, 'ep', split_axis=1, concat_axis=1, tiled=True)  4.6 us
  transfers between devices with their start and end apart: 5, of which 4 were waited for; matrix products, arithmetic and copies ran while one was open for 17% of the time, Pallas kernels for 0%

commit v1 on v0

--- a/solution.py
+++ b/solution.py
@@ -1,6 +1,10 @@
+import functools
+
 import jax
 import jax.numpy as jnp
 from jax import lax
+from jax.experimental import pallas as pl
+from jax.experimental.pallas import tpu as pltpu
 from jax.sharding import PartitionSpec as P
 
 windows = (2, 4, 8, 16)
@@ -135,23 +139,452 @@
     return (mix_out, exp_out)
 
 
+lanes = 128
+MESH = pl.DeviceIdType.MESH
+f32 = jnp.float32
+bf16 = jnp.bfloat16
+
+
+def fused_kernel(
+    x_ref,
+    norm_ref,
+    routes_ref,
+    weights_ref,
+    mix_ref,
+    gain_ref,
+    groups_hbm,
+    branch_hbm,
+    gate_hbm,
+    up_hbm,
+    down_hbm,
+    mix_out,
+    exp_out,
+    wgu,
+    wd,
+    wb,
+    gw,
+    xn,
+    sb,
+    xg,
+    gu,
+    hid,
+    halo,
+    pooled,
+    keep_m,
+    ps_m,
+    pr_m,
+    xs_m,
+    xr_m,
+    keep,
+    ps,
+    pr,
+    xs,
+    xr,
+    zs,
+    zr,
+    w_sem,
+    d_send,
+    d_recv,
+    r_send,
+    r_recv,
+    z_send,
+    z_recv,
+    m_send,
+    m_recv,
+    h_sem,
+):
+    z = lax.axis_index("ep")
+    t = lax.axis_index("tp")
+    near = t + 1 - 2 * (t % 2)
+    across = (t + 2) % 4
+    diagonal = (near + 2) % 4
+    peers = [z, z + 1 - 2 * (z % 2), 3 - z, (z + 2) % 4]
+    tokens, width = x_ref.shape
+    quarter = width // 4
+    cap = xg.shape[2]
+    hid_tiles = gate_hbm.shape[2] // lanes
+    rows_mix, channels = mix_ref.shape
+    group_count = channels // lanes
+
+    loads = []
+    for i in range(2 * hid_tiles):
+        src = gate_hbm if i < hid_tiles else up_hbm
+        at = (i % hid_tiles) * lanes
+        loads.append(
+            pltpu.make_async_copy(
+                src.at[0, :, pl.ds(at, lanes)],
+                wgu.at[i // 2, :, pl.ds((i % 2) * lanes, lanes)],
+                w_sem.at[i],
+            )
+        )
+    n0 = 2 * hid_tiles
+    load_b = [
+        pltpu.make_async_copy(branch_hbm.at[:, pl.ds(k * quarter, quarter)], wb.at[k], w_sem.at[n0 + k])
+        for k in range(4)
+    ]
+    load_d = [
+        pltpu.make_async_copy(down_hbm.at[0, :, pl.ds(k * quarter, quarter)], wd.at[k], w_sem.at[n0 + 4 + k])
+        for k in range(4)
+    ]
+    load_g = pltpu.make_async_copy(groups_hbm.at[pl.ds(t * group_count, group_count)], gw, w_sem.at[n0 + 8])
+    load_g.start()
+    for c in load_b + loads + load_d:
+        c.start()
+
+    barrier = pltpu.get_barrier_semaphore()
+    for k in (1, 2, 3):
+        pl.semaphore_signal(barrier, inc=1, device_id={"ep": peers[k]}, device_id_type=MESH)
+    for k in (near, across):
+        pl.semaphore_signal(barrier, inc=1, device_id={"tp": k}, device_id_type=MESH)
+
+    def remote(src, dst, send, recv, who):
+        return pltpu.make_async_remote_copy(
+            src_ref=src, dst_ref=dst, send_sem=send, recv_sem=recv, device_id=who, device_id_type=MESH
+        )
+
+    floated = x_ref[...].astype(f32)
+    scale = lax.rsqrt(jnp.mean(floated * floated, axis=1, keepdims=True) + epsilon)
+    xn_val = (floated * scale * norm_ref[...]).astype(bf16)
+    for k in range(4):
+        xn[k] = xn_val[:, k * quarter : (k + 1) * quarter]
+    r0 = routes_ref[:, 0:1]
+    r1 = routes_ref[:, 1:2]
+    lane = lax.broadcasted_iota(jnp.int32, (tokens, lanes), 1)
+    member = ((r0 == lane) | (r1 == lane)).astype(f32)
+    above = (
+        lax.broadcasted_iota(jnp.int32, (tokens, tokens), 0)
+        > lax.broadcasted_iota(jnp.int32, (tokens, tokens), 1)
+    ).astype(f32)
+    rank = jnp.dot(above.astype(bf16), member.astype(bf16), preferred_element_type=f32)
+    slot_lane = lax.broadcasted_iota(jnp.int32, (tokens, cap), 1)
+    places = []
+    shares = []
+    for k in range(4):
+        own = jnp.sum(jnp.where(lane == peers[k], rank, 0.0), axis=1, keepdims=True).astype(jnp.int32)
+        named = (r0 == peers[k]) | (r1 == peers[k])
+        slot = jnp.where(named, own, cap)
+        places.append((slot_lane == slot).astype(f32).astype(bf16))
+        shares.append(
+            jnp.where(r0 == peers[k], weights_ref[:, 0:1], 0.0)
+            + jnp.where(r1 == peers[k], weights_ref[:, 1:2], 0.0)
+        )
+
+    def gathered(k, block):
+        return lax.dot_general(
+            places[k], block, (((0,), (0,)), ((), ())), preferred_element_type=f32
+        ).astype(bf16)
+
+    own_cols = xn[t]
+    for k in (1, 2, 3):
+        sb[k] = gathered(k, own_cols)
+    pl.semaphore_wait(barrier, 5)
+    d_z = []
+    for k in (1, 2, 3):
+        c = remote(sb.at[k], xg.at[t, k], d_send.at[k - 1, 0], d_recv.at[k - 1, 0], {"ep": peers[k]})
+        c.start()
+        d_z.append(c)
+    halo_copy = remote(
+        mix_ref.at[pl.ds(rows_mix - 16, 16), :], halo, h_sem.at[0], h_sem.at[1], {"ep": (z + 1) % 4}
+    )
+
+    @pl.when(z < 3)
+    def _():
+        halo_copy.start()
+
+    for q in range(4):
+        xg[q, 0] = gathered(0, xn[q])
+
+    @pl.when(z == 0)
+    def _():
+        halo[...] = jnp.zeros_like(halo)
+
+    @pl.when(z > 0)
+    def _():
+        halo_copy.wait_recv()
+
+    load_g.wait()
+    position = z * rows_mix + lax.broadcasted_iota(jnp.int32, (rows_mix, lanes), 0)
+    for g in range(group_count):
+        cols = slice(g * lanes, (g + 1) * lanes)
+        current = mix_ref[:, cols].astype(f32)
+        total = jnp.concatenate([halo[:, cols].astype(f32), current], axis=0)
+        level = g % 4
+        for step in range(level + 1):
+            total = total + pltpu.roll(total, 1 << step, 0)
+        counted = jnp.minimum(position + 1, windows[level]).astype(f32)
+        deviation = (total[16:] / counted - current).astype(bf16)
+        grouped = jnp.dot(deviation, gw[g], preferred_element_type=f32)
+        gain = gain_ref[:, pl.ds(pl.multiple_of(t * channels + g * lanes, lanes), lanes)]
+        pooled[:, cols] = (grouped * gain).astype(bf16)
+    for c in load_b:
+        c.wait()
+
+    m_p = []
+    for i, q in enumerate((diagonal, near)):
+        ps_m[i] = jnp.dot(pooled[...], wb[q], preferred_element_type=f32).astype(bf16)
+        c = remote(ps_m.at[i], pr_m.at[i], m_send.at[i], m_recv.at[i], {"tp": near})
+        c.start()
+        m_p.append(c)
+    for i, q in enumerate((across, t)):
+        keep_m[i] = jnp.dot(pooled[...], wb[q], preferred_element_type=f32)
+
+    d_x = [
+        remote(xg.at[t, k], xg.at[t, k], d_send.at[k - 1, 1], d_recv.at[k - 1, 1], {"tp": across})
+        for k in (1, 2, 3)
+    ]
+    d_p = [
+        remote(xg.at[t, k], xg.at[t, k], d_send.at[k - 1, 2], d_recv.at[k - 1, 2], {"tp": near})
+        for k in (1, 2, 3)
+    ]
+    d_q = [
+        remote(xg.at[across, k], xg.at[across, k], d_send.at[k - 1, 3], d_recv.at[k - 1, 3], {"tp": near})
+        for k in (1, 2, 3)
+    ]
+
+    def from_z(k):
+        d_z[k - 1].wait_recv()
+        d_x[k - 1].start()
+        d_p[k - 1].start()
+
+    def from_x(k):
+        d_x[k - 1].wait_recv()
+        d_q[k - 1].start()
+
+    def from_near(k):
+        d_p[k - 1].wait_recv()
+        d_q[k - 1].wait_recv()
+
+    def expand(h):
+        def tile(n, carry):
+            total = None
+            for q in range(4):
+                part = jnp.dot(
+                    xg[q, 2 * h : 2 * h + 2].reshape(2 * cap, quarter),
+                    wgu[n, q * quarter : (q + 1) * quarter, :],
+                    preferred_element_type=f32,
+                )
+                total = part if total is None else total + part
+            gu[n] = total
+            return carry
+
+        lax.fori_loop(0, hid_tiles, tile, 0)
+        for i in range(hid_tiles):
+            k = hid_tiles + i
+            gate = gu[i // 2, :, (i % 2) * lanes : (i % 2 + 1) * lanes]
+            up = gu[k // 2, :, (k % 2) * lanes : (k % 2 + 1) * lanes]
+            hid[h, :, i * lanes : (i + 1) * lanes] = (gate / (1.0 + jnp.exp(-gate)) * up).astype(bf16)
+
+    r_p = [
+        [
+            remote(ps.at[i, k], pr.at[i, k], r_send.at[i, k], r_recv.at[i, k], {"tp": near})
+            for k in range(4)
+        ]
+        for i in range(2)
+    ]
+    r_x = [
+        remote(xs.at[k], xr.at[k], r_send.at[2, k], r_recv.at[2, k], {"tp": across}) for k in range(4)
+    ]
+    r_z = [
+        remote(zs.at[k], zr.at[k], z_send.at[k], z_recv.at[k], {"ep": peers[k]}) for k in range(4)
+    ]
+
+    def project(h):
+        for i, q in enumerate((diagonal, across, near, t)):
+            part = jnp.dot(hid[h], wd[q], preferred_element_type=f32)
+            for b in range(2):
+                k = 2 * h + b
+                piece = part[b * cap : (b + 1) * cap]
+                if i % 2 == 0:
+                    ps[i // 2, k] = piece.astype(bf16)
+                    r_p[i // 2][k].start()
+                else:
+                    keep[i // 2, k] = piece
+
+    def send_x(k):
+        r_p[0][k].wait_recv()
+        xs[k] = (keep[0, k] + pr[0, k].astype(f32)).astype(bf16)
+        r_x[k].start()
+
+    def send_z(k):
+        r_p[1][k].wait_recv()
+        r_x[k].wait_recv()
+        zs[k] = (keep[1, k] + pr[1, k].astype(f32) + xr[k].astype(f32)).astype(bf16)
+        if k > 0:
+            r_z[k].start()
+
+    from_z(1)
+    from_z(2)
+    from_x(1)
+    for c in loads:
+        c.wait()
+    from_near(1)
+    expand(0)
+    from_x(2)
+    from_z(3)
+    m_p[0].wait_recv()
+    xs_m[...] = (keep_m[0] + pr_m[0].astype(f32)).astype(bf16)
+    m_x = remote(xs_m, xr_m, m_send.at[2], m_recv.at[2], {"tp": across})
+    from_x(3)
+    m_x.start()
+    from_near(2)
+    from_near(3)
+    expand(1)
+    for c in load_d:
+        c.wait()
+    project(1)
+    send_x(2)
+    send_x(3)
+    project(0)
+    send_x(1)
+    send_x(0)
+    send_z(2)
+    send_z(3)
+    send_z(1)
+    m_p[1].wait_recv()
+    m_x.wait_recv()
+    mix_out[...] = (keep_m[1] + pr_m[1].astype(f32) + xr_m[...].astype(f32)).astype(bf16)
+    send_z(0)
+
+    result = jnp.zeros((tokens, quarter), f32)
+    for k in (0, 1, 2, 3):
+        if k > 0:
+            r_z[k].wait_recv()
+        block = zs[0] if k == 0 else zr[k]
+        result = result + shares[k] * jnp.dot(places[k], block, preferred_element_type=f32)
+    exp_out[...] = result.astype(bf16)
+
+    @pl.when(z < 3)
+    def _():
+        halo_copy.wait_send()
+
+    for c in d_z + d_x + d_p + d_q + r_p[0] + r_p[1] + r_x + r_z[1:] + m_p + [m_x]:
+        c.wait_send()
+
+
+def fused(
+    mix_input,
+    group_weight,
+    pool_gain,
+    branch_weight,
+    exp_input,
+    norm_gain,
+    routes,
+    route_weights,
+    gate_weight,
+    up_weight,
+    down_weight,
+):
+    tokens, width = exp_input.shape
+    rows_mix, channels = mix_input.shape
+    hidden = gate_weight.shape[2]
+    quarter = width // 4
+    cap = 3 * tokens // 4
+    hid_tiles = hidden // lanes
+    vmem = pl.BlockSpec(memory_space=pltpu.VMEM)
+    anywhere = pl.BlockSpec(memory_space=pl.ANY)
+    dma = pltpu.SemaphoreType.DMA
+    return pl.pallas_call(
+        fused_kernel,
+        out_shape=(
+            jax.ShapeDtypeStruct((rows_mix, quarter), bf16),
+            jax.ShapeDtypeStruct((tokens, quarter), bf16),
+        ),
+        in_specs=[vmem] * 6 + [anywhere] * 5,
+        out_specs=(vmem, vmem),
+        scratch_shapes=[
+            pltpu.VMEM((hid_tiles, width, 2 * lanes), bf16),
+            pltpu.VMEM((4, hidden, quarter), bf16),
+            pltpu.VMEM((4, channels, quarter), bf16),
+            pltpu.VMEM((channels // lanes, lanes, lanes), bf16),
+            pltpu.VMEM((4, tokens, quarter), bf16),
+            pltpu.VMEM((4, cap, quarter), bf16),
+            pltpu.VMEM((4, 4, cap, quarter), bf16),
+            pltpu.VMEM((hid_tiles, 2 * cap, 2 * lanes), f32),
+            pltpu.VMEM((2, 2 * cap, hidden), bf16),
+            pltpu.VMEM((16, channels), bf16),
+            pltpu.VMEM((rows_mix, channels), bf16),
+            pltpu.VMEM((2, rows_mix, quarter), f32),
+            pltpu.VMEM((2, rows_mix, quarter), bf16),
+            pltpu.VMEM((2, rows_mix, quarter), bf16),
+            pltpu.VMEM((rows_mix, quarter), bf16),
+            pltpu.VMEM((rows_mix, quarter), bf16),
+            pltpu.VMEM((2, 4, cap, quarter), f32),
+            pltpu.VMEM((2, 4, cap, quarter), bf16),
+            pltpu.VMEM((2, 4, cap, quarter), bf16),
+            pltpu.VMEM((4, cap, quarter), bf16),
+            pltpu.VMEM((4, cap, quarter), bf16),
+            pltpu.VMEM((4, cap, quarter), bf16),
+            pltpu.VMEM((4, cap, quarter), bf16),
+            dma((2 * hid_tiles + 9,)),
+            dma((3, 4)),
+            dma((3, 4)),
+            dma((3, 4)),
+            dma((3, 4)),
+            dma((4,)),
+            dma((4,)),
+            dma((3,)),
+            dma((3,)),
+            dma((2,)),
+        ],
+        compiler_params=pltpu.CompilerParams(
+            collective_id=0, has_side_effects=True, vmem_limit_bytes=56 << 20
+        ),
+    )(
+        exp_input,
+        norm_gain.reshape(1, -1),
+        routes,
+        route_weights,
+        mix_input,
+        pool_gain.reshape(1, -1),
+        group_weight,
+        branch_weight,
+        gate_weight,
+        up_weight,
+        down_weight,
+    )
+
+
+def fits(mesh, args):
+    mix, group, _, _, tok, _, routes, _, gate, _, _ = args
+    ep, tp, grp = (mesh.shape[k] for k in ("ep", "tp", "grp"))
+    if ep != 4 or tp != 4 or routes.shape[1] != 2 or gate.shape[0] != ep:
+        return False
+    rows, channels = mix.shape[0] // (grp * ep), mix.shape[1] // tp
+    tokens, quarter = tok.shape[0] // (grp * ep), tok.shape[1] // tp
+    return (
+        group.shape[1] == lanes
+        and channels % (4 * lanes) == 0
+        and channels == quarter
+        and rows % 16 == 0
+        and tokens % 64 == 0
+        and gate.shape[2] % (tp * lanes) == 0
+        and gate.shape[1] * gate.shape[2] <= 1 << 23
+        and rows <= 512
+        and tokens <= 256
+    )
+
+
 def solution(mesh):
-    return jax.shard_map(
-        on_device,
-        mesh=mesh,
-        in_specs=(
-            P(("grp", "ep"), "tp"),
-            P(),
-            P(),
-            P("tp", None),
-            P(("grp", "ep"), None),
-            P(),
-            P(("grp", "ep"), None),
-            P(("grp", "ep"), None),
-            P("ep", None, "tp"),
-            P("ep", None, "tp"),
-            P("ep", "tp", None),
-        ),
-        out_specs=(P(("grp", "ep"), "tp"), P(("grp", "ep"), "tp")),
-        check_vma=False,
-    )
+    def run(*args):
+        body = fused if fits(mesh, args) else on_device
+        return jax.shard_map(
+            body,
+            mesh=mesh,
+            in_specs=(
+                P(("grp", "ep"), "tp"),
+                P(),
+                P(),
+                P("tp", None),
+                P(("grp", "ep"), None),
+                P(),
+                P(("grp", "ep"), None),
+                P(("grp", "ep"), None),
+                P("ep", None, "tp"),
+                P("ep", None, "tp"),
+                P("ep", "tp", None),
+            ),
+            out_specs=(P(("grp", "ep"), "tp"), P(("grp", "ep"), "tp")),
+            check_vma=False,
+        )(*args)
+
+    return run

time: 131 us -> 56.3 us (0.43)
  waiting for transfers between devices: 60.4 us -> 0 us
  Pallas kernels: 0 us -> 49.4 us
  blocking collectives: 17.9 us -> 0 us
  matrix products: 17.2 us -> 0 us
  between operations: 14 us -> 0.64 us
  starting transfers between devices: 6.83 us -> 0 us
  other arithmetic: 6.43 us -> 0 us
  local copies, waits for them, and re-layouts: 7.86 us -> 6.06 us
    pallas_call x0 -> x1, Pallas kernels: none -> 49.4 us  [fused(): pl.pallas_call(fused_kernel, out_shape=(jax.ShapeDtypeStruct((rows_mix, q...]
    reduce_scatter x2 -> x0, waiting for transfers between devices: 32.3 us -> none  [the longest x1 23.4 us: on_device(): lax.psum_scatter(lax.dot_general(weight_cols, hidden, (((0,), (1,)), ((),...]
    all_to_all x1 -> x0, blocking collectives: 17.9 us -> none  [on_device(): lax.all_to_all(outgoing, 'ep', split_axis=0, concat_axis=0, tiled=True)]
    dot_general x4 -> x0, matrix products: 17.2 us -> none  [the longest x1 8.61 us: on_device(): lax.dot_general(weight_cols, hidden, (((0,), (1,)), ((), ())), preferred_...]
    all_gather x1 -> x0, waiting for transfers between devices: 16.7 us -> none  [on_device(): section = lax.all_gather(arrived, 'tp', axis=1, tiled=True)]
    all_to_all x1 -> x0, waiting for transfers between devices: 11.4 us -> none  [on_device(): lax.all_to_all(results, 'ep', split_axis=1, concat_axis=1, tiled=True)]
    unnamed x8 -> x4, local copies, waits for them, and re-layouts: 1.06 us -> 6.06 us
    all_to_all x1 -> x0, starting transfers between devices: 4.6 us -> none  [on_device(): lax.all_to_all(results, 'ep', split_axis=1, concat_axis=1, tiled=True)]
  transfers between devices with their start and end apart: 5 -> 0, of which waited for: 4 -> 0; matrix products, arithmetic and copies ran while one was open for 17% -> 0% of each run, Pallas kernels for 0% -> 0%
where the time goes in v1:
time: 56.3 us; the launch traced here: 56.1 us
  Pallas kernels  49.4 us (88%)
  local copies, waits for them, and re-layouts  6.06 us (11%)
  between operations  0.64 us (1%)
    pallas_call x1, Pallas kernels, fused(): pl.pallas_call(fused_kernel, out_shape=(jax.ShapeDtypeStruct((rows_mix, q...  49.4 us
    unnamed x4, local copies, waits for them, and re-layouts  6.06 us

profile of v1, /device:TPU:0, one launch (start us, length us, event | category | flops | bytes accessed | tf_op | source)
XLA Modules:
  0.0 56.1 jit_solution(3268158950823631119)
XLA Ops:
  0.6 1.4 %copy.13.routes_ref = s32[128,2]{1,0:T(8,128)} copy(s32[128,2]{0,1:T(2,128)} %param.17) | data formatting | bytes 2048 | tf_op args[6]
  2.0 1.4 %copy.14.weights_ref = f32[128,2]{1,0:T(8,128)} copy(f32[128,2]{0,1:T(2,128)} %param.18) | data formatting | bytes 2048 | tf_op args[7]
  3.5 49.4 %shard_map.122 = (bf16[256,512]{1,0:T(8,128)(2,1)}, bf16[128,512]{1,0:T(8,128)(2,1)}) custom-call(bf16[128,2048]{1,0:T(8,128)(2,1)} %x_ref.1, f32[1,2048]{1,0:T(1,128)} %bitcast.2, s32[128,2]{1,0:T(8,128)} %copy.13.routes_ref, f32[128,2]{1,0:T(8,128)} %copy.14.weights_ref, bf16[256,512]{1,0:T(8,128)(2,1)} %mix_ref.1, f32[1,2048]{1,0:T(1,128)} %bitcast.3, ...), custom_call_target="tpu_custom_call" | custom-call | tf_op jit(solution)/shard_map/pallas_call | solution.py:486
  52.9 1.7 %copy.17 = bf16[256,512]{1,0:T(8,128)(2,1)} copy(bf16[256,512]{1,0:T(8,128)(2,1)} %get-tuple-element.4) | data formatting | bytes 524288
  54.5 1.6 %copy.18 = bf16[128,512]{1,0:T(8,128)(2,1)} copy(bf16[128,512]{1,0:T(8,128)(2,1)} %get-tuple-element.5) | data formatting | bytes 262144

commit v2 on v1

--- a/solution.py
+++ b/solution.py
@@ -247,9 +247,18 @@
     xn_val = (floated * scale * norm_ref[...]).astype(bf16)
     for k in range(4):
         xn[k] = xn_val[:, k * quarter : (k + 1) * quarter]
-    r0 = routes_ref[:, 0:1]
-    r1 = routes_ref[:, 1:2]
     lane = lax.broadcasted_iota(jnp.int32, (tokens, lanes), 1)
+    square = (tokens, tokens)
+    diagonal_mask = lax.broadcasted_iota(jnp.int32, square, 0) == lax.broadcasted_iota(jnp.int32, square, 1)
+
+    def column(row):
+        spread = jnp.broadcast_to(row, square)
+        return jnp.sum(jnp.where(diagonal_mask, spread, jnp.zeros_like(spread)), axis=1, keepdims=True)
+
+    r0 = column(routes_ref[0:1, :].astype(f32)).astype(jnp.int32)
+    r1 = column(routes_ref[1:2, :].astype(f32)).astype(jnp.int32)
+    w0 = column(weights_ref[0:1, :])
+    w1 = column(weights_ref[1:2, :])
     member = ((r0 == lane) | (r1 == lane)).astype(f32)
     above = (
         lax.broadcasted_iota(jnp.int32, (tokens, tokens), 0)
@@ -265,8 +274,8 @@
         slot = jnp.where(named, own, cap)
         places.append((slot_lane == slot).astype(f32).astype(bf16))
         shares.append(
-            jnp.where(r0 == peers[k], weights_ref[:, 0:1], 0.0)
-            + jnp.where(r1 == peers[k], weights_ref[:, 1:2], 0.0)
+            jnp.where(r0 == peers[k], w0, 0.0)
+            + jnp.where(r1 == peers[k], w1, 0.0)
         )
 
     def gathered(k, block):
@@ -278,19 +287,19 @@
     for k in (1, 2, 3):
         sb[k] = gathered(k, own_cols)
     pl.semaphore_wait(barrier, 5)
+    halo_copy = remote(
+        mix_ref.at[pl.ds(rows_mix - 16, 16), :], halo, h_sem.at[0], h_sem.at[1], {"ep": (z + 1) % 4}
+    )
+
+    @pl.when(z < 3)
+    def _():
+        halo_copy.start()
+
     d_z = []
     for k in (1, 2, 3):
         c = remote(sb.at[k], xg.at[t, k], d_send.at[k - 1, 0], d_recv.at[k - 1, 0], {"ep": peers[k]})
         c.start()
         d_z.append(c)
-    halo_copy = remote(
-        mix_ref.at[pl.ds(rows_mix - 16, 16), :], halo, h_sem.at[0], h_sem.at[1], {"ep": (z + 1) % 4}
-    )
-
-    @pl.when(z < 3)
-    def _():
-        halo_copy.start()
-
     for q in range(4):
         xg[q, 0] = gathered(0, xn[q])
 
@@ -354,7 +363,7 @@
         d_p[k - 1].wait_recv()
         d_q[k - 1].wait_recv()
 
-    def expand(h):
+    def expand(h, first, last):
         def tile(n, carry):
             total = None
             for q in range(4):
@@ -367,7 +376,9 @@
             gu[n] = total
             return carry
 
-        lax.fori_loop(0, hid_tiles, tile, 0)
+        lax.fori_loop(first, last, tile, 0)
+
+    def activate(h):
         for i in range(hid_tiles):
             k = hid_tiles + i
             gate = gu[i // 2, :, (i % 2) * lanes : (i % 2 + 1) * lanes]
@@ -412,45 +423,54 @@
         if k > 0:
             r_z[k].start()
 
+    half = hid_tiles // 2
     from_z(1)
     from_z(2)
     from_x(1)
     for c in loads:
         c.wait()
     from_near(1)
-    expand(0)
+    expand(0, 0, half)
     from_x(2)
     from_z(3)
+    expand(0, half, hid_tiles)
+    activate(0)
+    for c in load_d:
+        c.wait()
+    project(0)
+    from_x(3)
+    send_x(1)
+    send_x(0)
+    from_near(2)
+    from_near(3)
+    expand(1, 0, hid_tiles)
+    activate(1)
+    project(1)
+    send_x(2)
+    send_x(3)
     m_p[0].wait_recv()
     xs_m[...] = (keep_m[0] + pr_m[0].astype(f32)).astype(bf16)
     m_x = remote(xs_m, xr_m, m_send.at[2], m_recv.at[2], {"tp": across})
-    from_x(3)
     m_x.start()
-    from_near(2)
-    from_near(3)
-    expand(1)
-    for c in load_d:
-        c.wait()
-    project(1)
-    send_x(2)
-    send_x(3)
-    project(0)
-    send_x(1)
-    send_x(0)
+    send_z(1)
+    send_z(0)
     send_z(2)
     send_z(3)
-    send_z(1)
     m_p[1].wait_recv()
+    mix_sum = keep_m[1] + pr_m[1].astype(f32)
+
+    def share(k):
+        block = zs[0] if k == 0 else zr[k]
+        return shares[k] * jnp.dot(places[k], block, preferred_element_type=f32)
+
+    result = share(0)
+    r_z[1].wait_recv()
+    result = result + share(1)
     m_x.wait_recv()
-    mix_out[...] = (keep_m[1] + pr_m[1].astype(f32) + xr_m[...].astype(f32)).astype(bf16)
-    send_z(0)
-
-    result = jnp.zeros((tokens, quarter), f32)
-    for k in (0, 1, 2, 3):
-        if k > 0:
-            r_z[k].wait_recv()
-        block = zs[0] if k == 0 else zr[k]
-        result = result + shares[k] * jnp.dot(places[k], block, preferred_element_type=f32)
+    mix_out[...] = (mix_sum + xr_m[...].astype(f32)).astype(bf16)
+    for k in (2, 3):
+        r_z[k].wait_recv()
+        result = result + share(k)
     exp_out[...] = result.astype(bf16)
 
     @pl.when(z < 3)
@@ -486,8 +506,8 @@
     return pl.pallas_call(
         fused_kernel,
         out_shape=(
-            jax.ShapeDtypeStruct((rows_mix, quarter), bf16),
-            jax.ShapeDtypeStruct((tokens, quarter), bf16),
+            pltpu.VMEM((rows_mix, quarter), bf16),
+            pltpu.VMEM((tokens, quarter), bf16),
         ),
         in_specs=[vmem] * 6 + [anywhere] * 5,
         out_specs=(vmem, vmem),
@@ -532,8 +552,8 @@
     )(
         exp_input,
         norm_gain.reshape(1, -1),
-        routes,
-        route_weights,
+        routes.T,
+        route_weights.T,
         mix_input,
         pool_gain.reshape(1, -1),
         group_weight,

time: 56.3 us -> 45.3 us (0.80)
  Pallas kernels: 49.4 us -> 43.2 us
  local copies, waits for them, and re-layouts: 6.06 us -> 1.36 us
    pallas_call x1, Pallas kernels: 49.4 us -> 43.2 us  [fused(): pl.pallas_call(fused_kernel, out_shape=(pltpu.VMEM((rows_mix, quarter), b...]
    unnamed x4 -> x2, local copies, waits for them, and re-layouts: 6.06 us -> 1.36 us
where the time goes in v2:
time: 45.3 us; the launch traced here: 45.2 us
  Pallas kernels  43.2 us (95%)
  local copies, waits for them, and re-layouts  1.36 us (3%)
  between operations  0.64 us (1%)
    pallas_call x1, Pallas kernels, fused(): pl.pallas_call(fused_kernel, out_shape=(pltpu.VMEM((rows_mix, quarter), b...  43.2 us
    unnamed x2, local copies, waits for them, and re-layouts  1.36 us

profile of v2, /device:TPU:0, one launch (start us, length us, event | category | flops | bytes accessed | tf_op | source)
XLA Modules:
  0.0 45.2 jit_solution(12959453376015378795)
XLA Ops:
  0.6 43.2 %shard_map.122 = (bf16[256,512]{1,0:T(8,128)(2,1)S(1)}, bf16[128,512]{1,0:T(8,128)(2,1)S(1)}) custom-call(bf16[128,2048]{1,0:T(8,128)(2,1)} %x_ref.1, f32[1,2048]{1,0:T(1,128)} %bitcast.4, s32[2,128]{1,0:T(2,128)} %bitcast.6, f32[2,128]{1,0:T(2,128)} %bitcast.7, bf16[256,512]{1,0:T(8,128)(2,1)} %mix_ref.1, f32[1,2048]{1,0:T(1,128)} %bitcast.5, ...), custom_call_target="tpu_custom_call" | custom-call | tf_op jit(solution)/shard_map/pallas_call | solution.py:506
  43.8 0.7 %copy.15 = bf16[256,512]{1,0:T(8,128)(2,1)} copy(bf16[256,512]{1,0:T(8,128)(2,1)S(1)} %get-tuple-element.2) | data formatting | bytes 524288
  44.5 0.7 %copy.16 = bf16[128,512]{1,0:T(8,128)(2,1)} copy(bf16[128,512]{1,0:T(8,128)(2,1)S(1)} %get-tuple-element.3) | data formatting | bytes 262144
